TPU v7x, 32 devices: a whole 2x2x4 slice. The times are simulated.
32 devices in a mesh: sp: 8 (over z, core), tp: 4 (over y, x).
Axes of the slice: x: 2, y: 2, z: 4, core: 2. Of those that a mesh axis runs over, the one named last changes fastest.
Arguments:
- tokens: bfloat16 [8192, 4096], P('sp', 'tp'), may hold values from -6 to 6
- key_weight: bfloat16 [4096, 1024], P(None, 'tp'), may hold values from -0.005859375 to 0.005859375
- value_weight: bfloat16 [4096, 2048], P(None, 'tp'), may hold values from -0.09375 to 0.09375
- decay_weight: bfloat16 [2, 4096, 1024], P(None, None, 'tp'), may hold values from -0.09375 to 0.09375
- decay_bias: float32 [2, 1024], P(None, 'tp')
- decay_shift: float32 [8192, 16], P('sp', 'tp'), may hold values from -0.65 to 0
- new_query: bfloat16 [16, 64], P('tp'), may hold values from -6 to 6
- new_key: bfloat16 [16, 64], P('tp'), may hold values from -6 to 6
- new_value: bfloat16 [16, 128], P('tp'), may hold values from -6 to 6
- out_gain: float32 [128], replicated, may hold values from 0.1 to 1.9
Outputs:
- state_cache: bfloat16 [2, 16, 64, 128], P(None, 'tp', 'sp')
- decode_read: bfloat16 [16, 128], P('tp')
All inputs are finite; a program needn't handle non-finite values.
Results may differ from a plain program's by a relative error of at most 0.0039.
Values may be sent and summed in bfloat16 or wider, within the bound.
A program may use at most 64 MiB of HBM per device.

v0:
```python
import functools

import jax
import jax.numpy as jnp
from jax import lax
from jax.experimental import pallas as pl
from jax.experimental.pallas import tpu as pltpu
from jax.sharding import PartitionSpec as P

DK = 64
DV = 128
CHUNK = 128

gate_norm = 16.0
norm_epsilon = 1e-06

MESH = pl.DeviceIdType.MESH


def flipped(index, bits, d):
    out = index
    for b in bits:
        if d & b:
            out = out + b - 2 * b * lax.rem(lax.div(index, b), 2)
    return out


def kernel(
    n_sp,
    n_tp,
    tokens,
    kw,
    vw,
    dw,
    bias,
    shift,
    query,
    new_key,
    new_value,
    gain,
    state_out,
    read_out,
    tok_buf,
    kw_buf,
    vw_buf,
    dw_buf,
    acc_k,
    acc_v,
    acc_d,
    s_fwd,
    s_bwd,
    tot_own,
    tot_buf,
    st_send,
    st_recv,
    rd_send,
    rd_recv,
    local_sem,
    w_sem,
    own_send_sem,
    relay_send_sem,
    recv_sem,
    tot_send_sem,
    tot_recv_sem,
    st_send_sem,
    st_recv_sem,
    rd_send_sem,
    rd_recv_sem,
):
    sp = lax.axis_index("sp")
    tp = lax.axis_index("tp")
    bits = [1 << i for i in range(n_tp.bit_length() - 1)]
    order = sorted(range(n_tp), key=lambda d: (bin(d).count("1"), d))
    level = [bin(d).count("1") for d in order]
    place = {d: i for i, d in enumerate(order)}
    direct = [i for i in range(n_tp) if level[i] == 1]
    near = sum(1 for lv in level if lv <= 1)

    t_count, feat = tokens.shape
    rows = min(CHUNK, t_count)
    half = rows // 2
    chunks = t_count // rows
    width = kw.shape[1]
    heads = width // DK
    pair = 2 if heads % 2 == 0 else 1
    groups = heads // pair
    lanes = pair * DK
    r_count = DK // n_sp

    local = []
    for i, d in enumerate(order):
        src = pl.ds(pl.multiple_of(flipped(tp, bits, d) * feat, feat), feat)
        dst = pl.ds(i * feat, feat)
        local.append(pltpu.make_async_copy(kw.at[src], kw_buf.at[dst], w_sem.at[i, 0]))
        local.append(pltpu.make_async_copy(vw.at[src], vw_buf.at[dst], w_sem.at[i, 1]))
        for k in range(2):
            local.append(
                pltpu.make_async_copy(dw.at[k, src], dw_buf.at[k, dst], w_sem.at[i, 2 + k])
            )
    local.append(pltpu.make_async_copy(tokens, tok_buf.at[0], local_sem.at[0]))

    barrier = pltpu.get_barrier_semaphore()
    for b in bits:
        pl.semaphore_signal(
            barrier, inc=1, device_id=(sp, flipped(tp, bits, b)), device_id_type=MESH
        )
    for d in range(1, n_sp):
        pl.semaphore_signal(
            barrier, inc=1, device_id=(lax.rem(sp + d, n_sp), tp), device_id_type=MESH
        )
    pl.semaphore_wait(barrier, len(bits) + n_sp - 1)

    def part(c, h):
        if h is None:
            return pl.ds(pl.multiple_of(c * rows, rows), rows)
        return pl.ds(pl.multiple_of(c * rows + h * half, half), half)

    def own_copy(c, j):
        b = bits[j]
        rs = part(c, None)
        return pltpu.make_async_remote_copy(
            src_ref=tokens.at[rs],
            dst_ref=tok_buf.at[place[b], rs],
            send_sem=own_send_sem.at[j, c],
            recv_sem=recv_sem.at[place[b], c, 0],
            device_id=(sp, flipped(tp, bits, b)),
            device_id_type=MESH,
        )

    relays = []
    for d in order[1:]:
        for b in bits:
            if not d & b:
                if b > d:
                    relays.append((d, 0, b))
                if all(b < o for o in bits if d & o):
                    relays.append((d, 1, b))

    def relay_copy(c, n):
        d, h, b = relays[n]
        rs = part(c, h)
        return pltpu.make_async_remote_copy(
            src_ref=tok_buf.at[place[d], rs],
            dst_ref=tok_buf.at[place[d | b], rs],
            send_sem=relay_send_sem.at[n, c],
            recv_sem=recv_sem.at[place[d | b], c, h],
            device_id=(sp, flipped(tp, bits, b)),
            device_id_type=MESH,
        )

    def send_own(c):
        for j in range(len(bits)):
            own_copy(c, j).start()

    def wait_direct(c):
        for j in range(len(bits)):
            own_copy(c, j).wait_recv()

    def relay_level(c, lv):
        for n, (d, h, b) in enumerate(relays):
            if bin(d).count("1") == lv:
                relay_copy(c, n).start()

    def wait_level(c, lv):
        for n, (d, h, b) in enumerate(relays):
            if bin(d | b).count("1") == lv:
                relay_copy(c, n).wait_recv()

    for c in range(min(2, chunks)):
        send_own(c)
    for copy in local:
        copy.start()

    s_fwd[...] = jnp.zeros_like(s_fwd)
    s_bwd[...] = jnp.zeros_like(s_bwd)
    tot_own[...] = jnp.zeros_like(tot_own)

    t_ids = lax.broadcasted_iota(jnp.int32, (rows, 2 * rows), 0)
    s_ids = lax.broadcasted_iota(jnp.int32, (rows, 2 * rows), 1)
    s_ids = jnp.where(s_ids >= rows, s_ids - rows, s_ids)
    after = jnp.where(s_ids > t_ids, 1.0, 0.0).astype(jnp.bfloat16)
    before = jnp.where(s_ids < t_ids, 1.0, 0.0).astype(jnp.bfloat16)
    first_head = lax.broadcasted_iota(jnp.int32, (DV, lanes), 1) < DK
    first_head_rows = lax.broadcasted_iota(jnp.int32, (rows, lanes), 1) < DK

    def dot(a, b):
        return jnp.dot(a, b, preferred_element_type=jnp.float32)

    def product(c, low, high):
        rs = part(c, None)
        x = jnp.concatenate([tok_buf[i, rs, :] for i in range(low, high)], axis=1)
        ws = slice(low * feat, high * feat)
        return (
            dot(x, kw_buf[ws, :]),
            dot(x, vw_buf[ws, :]),
            dot(x, dw_buf[0, ws, :]),
            dot(x, dw_buf[1, ws, :]),
        )

    def begin(c):
        p = lax.rem(c, 2)
        k, v, f, b = product(c, 0, near)
        acc_k[p] = k
        acc_v[p] = v
        acc_d[p, 0] = f
        acc_d[p, 1] = b

    def log_gate(pre, shift_wide):
        return (
            jnp.minimum(pre, 0.0) - jnp.log(1.0 + jnp.exp(-jnp.abs(pre)))
        ) * (1.0 / gate_norm) + shift_wide

    def summed(mask, log):
        hi = log.astype(jnp.bfloat16)
        lo = (log - hi.astype(jnp.float32)).astype(jnp.bfloat16)
        return dot(mask, jnp.concatenate([hi, lo], axis=0))

    def finish(c):
        p = lax.rem(c, 2)
        for lv in range(2, len(bits) + 1):
            wait_level(c, lv)
            relay_level(c, lv)
        k, v, f, b = acc_k[p], acc_v[p], acc_d[p, 0], acc_d[p, 1]
        if near < n_tp:
            more = product(c, near, n_tp)
            k, v, f, b = k + more[0], v + more[1], f + more[2], b + more[3]
        k = k.astype(jnp.bfloat16).astype(jnp.float32)
        v = v.astype(jnp.bfloat16)
        sh = shift[part(c, None), :]
        wide = []
        for g in range(groups):
            one = jnp.broadcast_to(sh[:, g * pair : g * pair + 1], (rows, lanes))
            if pair == 2:
                two = jnp.broadcast_to(sh[:, g * pair + 1 : g * pair + 2], (rows, lanes))
                one = jnp.where(first_head_rows, one, two)
            wide.append(one)
        shift_wide = wide[0] if groups == 1 else jnp.concatenate(wide, axis=1)
        f_log = log_gate(f + bias[0:1, :], shift_wide)
        b_log = log_gate(b + bias[1:2, :], shift_wide)
        f_total = jnp.sum(f_log, axis=0, keepdims=True)
        b_total = jnp.sum(b_log, axis=0, keepdims=True)
        f_keys = (k * jnp.exp(summed(after, f_log))).astype(jnp.bfloat16)
        b_keys = (k * jnp.exp(summed(before, b_log) + tot_own[1:2, :])).astype(jnp.bfloat16)
        f_scale = jnp.exp(f_total)
        tot_own[0:1, :] += f_total
        tot_own[1:2, :] += b_total

        def outer(v_group, keys):
            r = lax.dot_general(
                v_group, keys, (((0,), (0,)), ((), ())), preferred_element_type=jnp.float32
            )
            return jnp.where(first_head, r[:DV], r[DV:]) if pair == 2 else r

        for g in range(groups):
            cs = slice(g * lanes, (g + 1) * lanes)
            v_group = v[:, g * pair * DV : (g + 1) * pair * DV]
            s_fwd[:, cs] = s_fwd[:, cs] * f_scale[:, cs] + outer(v_group, f_keys[:, cs])
            s_bwd[:, cs] += outer(v_group, b_keys[:, cs])

    for copy in local:
        copy.wait()

    def step(c, carry):
        wait_direct(c)
        relay_level(c, 1)

        @pl.when(c + 2 < chunks)
        def _():
            send_own(c + 2)

        begin(c)

        @pl.when(c > 0)
        def _():
            finish(c - 1)

        return carry

    lax.fori_loop(0, chunks, step, 0)
    finish(chunks - 1)

    def peer(d):
        return lax.rem(sp + d, n_sp)

    def total_copy(d):
        return pltpu.make_async_remote_copy(
            src_ref=tot_own,
            dst_ref=tot_buf.at[sp],
            send_sem=tot_send_sem.at[d],
            recv_sem=tot_recv_sem.at[sp],
            device_id=(peer(d), tp),
            device_id_type=MESH,
        )

    for d in range(1, n_sp):
        total_copy(d).start()
    later = jnp.zeros((1, width), jnp.float32)
    earlier = jnp.zeros((1, width), jnp.float32)
    for d in range(1, n_sp):
        src = peer(d)
        pltpu.make_async_remote_copy(
            src_ref=tot_own,
            dst_ref=tot_buf.at[src],
            send_sem=tot_send_sem.at[d],
            recv_sem=tot_recv_sem.at[src],
            device_id=(src, tp),
            device_id_type=MESH,
        ).wait_recv()
        got = tot_buf[src]
        later += jnp.where(src > sp, got[0:1, :], 0.0)
        earlier += jnp.where(src < sp, got[1:2, :], 0.0)

    def upright(s):
        tiles = [s[:, g * lanes : (g + 1) * lanes].T for g in range(groups)]
        return tiles[0] if groups == 1 else jnp.concatenate(tiles, axis=0)

    w_fwd = upright(s_fwd[...] * jnp.exp(later))
    w_bwd = upright(s_bwd[...] * jnp.exp(earlier))
    for r in range(n_sp):
        for h in range(heads):
            rs = slice(h * DK + r * r_count, h * DK + (r + 1) * r_count)
            st_send[r, 0, h] = w_fwd[rs]
            st_send[r, 1, h] = w_bwd[rs]

    def state_copy(dst, slot, d):
        return pltpu.make_async_remote_copy(
            src_ref=st_send.at[dst],
            dst_ref=st_recv.at[slot],
            send_sem=st_send_sem.at[d],
            recv_sem=st_recv_sem.at[slot],
            device_id=(dst, tp),
            device_id_type=MESH,
        )

    def read_copy(dst, slot, d):
        return pltpu.make_async_remote_copy(
            src_ref=rd_send,
            dst_ref=rd_recv.at[slot],
            send_sem=rd_send_sem.at[d],
            recv_sem=rd_recv_sem.at[slot],
            device_id=(dst, tp),
            device_id_type=MESH,
        )

    for d in range(1, n_sp):
        state_copy(peer(d), sp, d).start()

    q = query[...].astype(jnp.float32)
    both = w_fwd + w_bwd
    head_ids = lax.broadcasted_iota(jnp.int32, (heads, DV), 0)
    read = jnp.zeros((heads, DV), jnp.float32)
    for h in range(heads):
        one = jnp.dot(
            q,
            both[h * DK : (h + 1) * DK],
            precision=lax.Precision.HIGHEST,
            preferred_element_type=jnp.float32,
        )
        read = jnp.where(head_ids == h, one, read)
    rd_send[...] = read
    for d in range(1, n_sp):
        read_copy(peer(d), sp, d).start()

    raw = read + jnp.sum(
        q * new_key[...].astype(jnp.float32), axis=-1, keepdims=True
    ) * new_value[...].astype(jnp.float32)
    for d in range(1, n_sp):
        read_copy(peer(d), peer(d), d).wait_recv()
        raw += rd_recv[peer(d)]
    scale = lax.rsqrt(jnp.mean(raw * raw, axis=-1, keepdims=True) + norm_epsilon)
    read_out[...] = (raw * scale * gain[...]).astype(jnp.bfloat16)

    state = st_send[sp]
    for d in range(1, n_sp):
        state_copy(peer(d), peer(d), d).wait_recv()
        state += st_recv[peer(d)]
    state_out[...] = state.astype(jnp.bfloat16)

    def drain(c, carry):
        for j in range(len(bits)):
            own_copy(c, j).wait_send()
        for n in range(len(relays)):
            relay_copy(c, n).wait_send()
        return carry

    lax.fori_loop(0, chunks, drain, 0)
    for d in range(1, n_sp):
        total_copy(d).wait_send()
        state_copy(peer(d), sp, d).wait_send()
        read_copy(peer(d), sp, d).wait_send()


def shards(
    n_sp,
    n_tp,
    tokens,
    key_weight,
    value_weight,
    decay_weight,
    decay_bias,
    decay_shift,
    new_query,
    new_key,
    new_value,
    out_gain,
):
    t_count, feat = tokens.shape
    depth, width = key_weight.shape
    v_width = value_weight.shape[1]
    heads = width // DK
    r_count = DK // n_sp
    rows = min(CHUNK, t_count)
    chunks = t_count // rows
    n_bits = n_tp.bit_length() - 1
    n_relays = n_tp * n_tp
    any_spec = pl.BlockSpec(memory_space=pl.ANY)
    vmem_spec = pl.BlockSpec(memory_space=pltpu.VMEM)
    dma = pltpu.SemaphoreType.DMA
    f32, bf16 = jnp.float32, jnp.bfloat16
    return pl.pallas_call(
        functools.partial(kernel, n_sp, n_tp),
        out_shape=(
            jax.ShapeDtypeStruct((2, heads, r_count, DV), bf16),
            jax.ShapeDtypeStruct((heads, DV), bf16),
        ),
        in_specs=[any_spec] * 4 + [vmem_spec] * 6,
        out_specs=(vmem_spec, vmem_spec),
        scratch_shapes=[
            pltpu.VMEM((n_tp, t_count, feat), bf16),
            pltpu.VMEM((depth, width), bf16),
            pltpu.VMEM((depth, v_width), bf16),
            pltpu.VMEM((2, depth, width), bf16),
            pltpu.VMEM((2, rows, width), f32),
            pltpu.VMEM((2, rows, v_width), f32),
            pltpu.VMEM((2, 2, rows, width), f32),
            pltpu.VMEM((DV, width), f32),
            pltpu.VMEM((DV, width), f32),
            pltpu.VMEM((2, width), f32),
            pltpu.VMEM((n_sp, 2, width), f32),
            pltpu.VMEM((n_sp, 2, heads, r_count, DV), f32),
            pltpu.VMEM((n_sp, 2, heads, r_count, DV), f32),
            pltpu.VMEM((heads, DV), f32),
            pltpu.VMEM((n_sp, heads, DV), f32),
            dma((1,)),
            dma((n_tp, 4)),
            dma((max(n_bits, 1), chunks)),
            dma((n_relays, chunks)),
            dma((n_tp, chunks, 2)),
            dma((n_sp,)),
            dma((n_sp,)),
            dma((n_sp,)),
            dma((n_sp,)),
            dma((n_sp,)),
            dma((n_sp,)),
        ],
        compiler_params=pltpu.CompilerParams(collective_id=0, has_side_effects=True),
    )(
        tokens,
        key_weight,
        value_weight,
        decay_weight,
        decay_bias,
        decay_shift,
        new_query,
        new_key,
        new_value,
        out_gain.reshape(1, DV),
    )


def solution(mesh):
    placed = (
        P("sp", "tp"),
        P(None, "tp"),
        P(None, "tp"),
        P(None, None, "tp"),
        P(None, "tp"),
        P("sp", "tp"),
        P("tp", None),
        P("tp", None),
        P("tp", None),
        P(),
    )
    return jax.shard_map(
        functools.partial(shards, mesh.shape["sp"], mesh.shape["tp"]),
        mesh=mesh,
        in_specs=placed,
        out_specs=(P(None, "tp", "sp", None), P("tp", None)),
        check_vma=False,
    )
```

profile of v0, /device:TPU:0, one launch (start us, length us, event | category | flops | bytes accessed | tf_op | source)
XLA Modules:
  0.0 97.0 jit_solution(3388333129713719935)
XLA Ops:
  0.6 1.7 %copy.12.shift = f32[1024,4]{1,0:T(8,128)} copy(f32[1024,4]{0,1:T(4,128)} %param.15) | data formatting | bytes 32768 | tf_op args[5]
  2.4 92.1 %shard_map.113 = (bf16[2,4,8,128]{3,2,1,0:T(8,128)(2,1)}, bf16[4,128]{1,0:T(4,128)(2,1)}) custom-call(bf16[1024,1024]{1,0:T(8,128)(2,1)} %tokens.1, bf16[4096,256]{1,0:T(8,128)(2,1)} %kw.1, bf16[4096,512]{1,0:T(8,128)(2,1)} %vw.1, bf16[2,4096,256]{2,1,0:T(8,128)(2,1)} %dw.1, f32[2,256]{1,0:T(2,128)} %bias.1, f32[1024,4]{1,0:T(8,128)} %copy.12.shift, ...), custom_call_target="tpu_custom_call" | custom-call | tf_op jit(solution)/shard_map/pallas_call | solution.py:420
  94.5 1.3 %copy.15 = bf16[2,4,8,128]{3,2,1,0:T(8,128)(2,1)} copy(bf16[2,4,8,128]{3,2,1,0:T(8,128)(2,1)} %get-tuple-element.4) | data formatting | bytes 32768
  95.8 1.2 %copy.16 = bf16[4,128]{1,0:T(4,128)(2,1)} copy(bf16[4,128]{1,0:T(4,128)(2,1)} %get-tuple-element.5) | data formatting | bytes 2048
where the time goes:
time: 97.4 us; the launch traced here: 97 us
  Pallas kernels  92.1 us (95%)
  local copies, waits for them, and re-layouts  4.28 us (4%)
    pallas_call x1, Pallas kernels, shards(): pl.pallas_call(functools.partial(kernel, n_sp, n_tp), out_shape=(jax.Shap...  92.1 us
    unnamed x3, local copies, waits for them, and re-layouts  4.28 us

commit v1 on v0

--- a/solution.py
+++ b/solution.py
@@ -32,14 +32,22 @@
     kw,
     vw,
     dw,
+    bias_in,
+    shift_in,
+    query_in,
+    new_key_in,
+    new_value_in,
+    gain_in,
+    state_out,
+    read_out,
     bias,
     shift,
     query,
     new_key,
     new_value,
     gain,
-    state_out,
-    read_out,
+    state_buf,
+    read_buf,
     tok_buf,
     kw_buf,
     vw_buf,
@@ -51,6 +59,7 @@
     s_bwd,
     tot_own,
     tot_buf,
+    st_own,
     st_send,
     st_recv,
     rd_send,
@@ -98,6 +107,18 @@
                 pltpu.make_async_copy(dw.at[k, src], dw_buf.at[k, dst], w_sem.at[i, 2 + k])
             )
     local.append(pltpu.make_async_copy(tokens, tok_buf.at[0], local_sem.at[0]))
+    small = (
+        (bias_in, bias),
+        (shift_in, shift),
+        (query_in, query),
+        (new_key_in, new_key),
+        (new_value_in, new_value),
+        (gain_in, gain),
+    )
+    for n, (src, dst) in enumerate(small):
+        local.append(pltpu.make_async_copy(src, dst, local_sem.at[1 + n]))
+    read_done = pltpu.make_async_copy(read_buf, read_out, local_sem.at[7])
+    state_done = pltpu.make_async_copy(state_buf, state_out, local_sem.at[8])
 
     barrier = pltpu.get_barrier_semaphore()
     for b in bits:
@@ -226,7 +247,7 @@
             k, v, f, b = k + more[0], v + more[1], f + more[2], b + more[3]
         k = k.astype(jnp.bfloat16).astype(jnp.float32)
         v = v.astype(jnp.bfloat16)
-        sh = shift[part(c, None), :]
+        sh = shift[:, part(c, None)].T
         wide = []
         for g in range(groups):
             one = jnp.broadcast_to(sh[:, g * pair : g * pair + 1], (rows, lanes))
@@ -319,8 +340,10 @@
     for r in range(n_sp):
         for h in range(heads):
             rs = slice(h * DK + r * r_count, h * DK + (r + 1) * r_count)
-            st_send[r, 0, h] = w_fwd[rs]
-            st_send[r, 1, h] = w_bwd[rs]
+            st_send[r, 0, h] = w_fwd[rs].astype(jnp.bfloat16)
+            st_send[r, 1, h] = w_bwd[rs].astype(jnp.bfloat16)
+            st_own[r, 0, h] = w_fwd[rs]
+            st_own[r, 1, h] = w_bwd[rs]
 
     def state_copy(dst, slot, d):
         return pltpu.make_async_remote_copy(
@@ -368,13 +391,15 @@
         read_copy(peer(d), peer(d), d).wait_recv()
         raw += rd_recv[peer(d)]
     scale = lax.rsqrt(jnp.mean(raw * raw, axis=-1, keepdims=True) + norm_epsilon)
-    read_out[...] = (raw * scale * gain[...]).astype(jnp.bfloat16)
-
-    state = st_send[sp]
+    read_buf[...] = (raw * scale * gain[...]).astype(jnp.bfloat16)
+    read_done.start()
+
+    state = st_own[sp]
     for d in range(1, n_sp):
         state_copy(peer(d), peer(d), d).wait_recv()
-        state += st_recv[peer(d)]
-    state_out[...] = state.astype(jnp.bfloat16)
+        state += st_recv[peer(d)].astype(jnp.float32)
+    state_buf[...] = state.astype(jnp.bfloat16)
+    state_done.start()
 
     def drain(c, carry):
         for j in range(len(bits)):
@@ -388,6 +413,8 @@
         total_copy(d).wait_send()
         state_copy(peer(d), sp, d).wait_send()
         read_copy(peer(d), sp, d).wait_send()
+    read_done.wait()
+    state_done.wait()
 
 
 def shards(
@@ -414,7 +441,6 @@
     n_bits = n_tp.bit_length() - 1
     n_relays = n_tp * n_tp
     any_spec = pl.BlockSpec(memory_space=pl.ANY)
-    vmem_spec = pl.BlockSpec(memory_space=pltpu.VMEM)
     dma = pltpu.SemaphoreType.DMA
     f32, bf16 = jnp.float32, jnp.bfloat16
     return pl.pallas_call(
@@ -423,9 +449,17 @@
             jax.ShapeDtypeStruct((2, heads, r_count, DV), bf16),
             jax.ShapeDtypeStruct((heads, DV), bf16),
         ),
-        in_specs=[any_spec] * 4 + [vmem_spec] * 6,
-        out_specs=(vmem_spec, vmem_spec),
+        in_specs=[any_spec] * 10,
+        out_specs=(any_spec, any_spec),
         scratch_shapes=[
+            pltpu.VMEM((2, width), f32),
+            pltpu.VMEM((heads, t_count), f32),
+            pltpu.VMEM((heads, DK), bf16),
+            pltpu.VMEM((heads, DK), bf16),
+            pltpu.VMEM((heads, DV), bf16),
+            pltpu.VMEM((1, DV), f32),
+            pltpu.VMEM((2, heads, r_count, DV), bf16),
+            pltpu.VMEM((heads, DV), bf16),
             pltpu.VMEM((n_tp, t_count, feat), bf16),
             pltpu.VMEM((depth, width), bf16),
             pltpu.VMEM((depth, v_width), bf16),
@@ -438,10 +472,11 @@
             pltpu.VMEM((2, width), f32),
             pltpu.VMEM((n_sp, 2, width), f32),
             pltpu.VMEM((n_sp, 2, heads, r_count, DV), f32),
-            pltpu.VMEM((n_sp, 2, heads, r_count, DV), f32),
+            pltpu.VMEM((n_sp, 2, heads, r_count, DV), bf16),
+            pltpu.VMEM((n_sp, 2, heads, r_count, DV), bf16),
             pltpu.VMEM((heads, DV), f32),
             pltpu.VMEM((n_sp, heads, DV), f32),
-            dma((1,)),
+            dma((9,)),
             dma((n_tp, 4)),
             dma((max(n_bits, 1), chunks)),
             dma((n_relays, chunks)),
@@ -460,7 +495,7 @@
         value_weight,
         decay_weight,
         decay_bias,
-        decay_shift,
+        decay_shift.T,
         new_query,
         new_key,
         new_value,

time: 97.4 us -> 91.9 us (0.944)
  Pallas kernels: 92.1 us -> 88.4 us
  local copies, waits for them, and re-layouts: 4.28 us -> 2.54 us
    pallas_call x1, Pallas kernels: 92.1 us -> 88.4 us  [shards(): pl.pallas_call(functools.partial(kernel, n_sp, n_tp), out_shape=(jax.Shap...]
    unnamed x3 -> x2, local copies, waits for them, and re-layouts: 4.28 us -> 2.54 us
where the time goes in v1:
time: 91.9 us; the launch traced here: 91.6 us
  Pallas kernels  88.4 us (96%)
  local copies, waits for them, and re-layouts  2.54 us (3%)
    pallas_call x1, Pallas kernels, shards(): pl.pallas_call(functools.partial(kernel, n_sp, n_tp), out_shape=(jax.Shap...  88.4 us
    unnamed x2, local copies, waits for them, and re-layouts  2.54 us

profile of v1, /device:TPU:0, one launch (start us, length us, event | category | flops | bytes accessed | tf_op | source)
XLA Modules:
  0.0 91.6 jit_solution(15213161161697218686)
XLA Ops:
  0.6 88.4 %shard_map.113 = (bf16[2,4,8,128]{3,2,1,0:T(8,128)(2,1)}, bf16[4,128]{1,0:T(4,128)(2,1)}) custom-call(bf16[1024,1024]{1,0:T(8,128)(2,1)} %tokens.1, bf16[4096,256]{1,0:T(8,128)(2,1)} %kw.1, bf16[4096,512]{1,0:T(8,128)(2,1)} %vw.1, bf16[2,4096,256]{2,1,0:T(8,128)(2,1)} %dw.1, f32[2,256]{1,0:T(2,128)} %bias_in.1, f32[4,1024]{1,0:T(4,128)} %bitcast.2, ...), custom_call_target="tpu_custom_call" | custom-call | tf_op jit(solution)/shard_map/pallas_call | solution.py:446
  89.1 1.3 %copy.14 = bf16[2,4,8,128]{3,2,1,0:T(8,128)(2,1)} copy(bf16[2,4,8,128]{3,2,1,0:T(8,128)(2,1)} %get-tuple-element.4) | data formatting | bytes 32768
  90.4 1.2 %copy.15 = bf16[4,128]{1,0:T(4,128)(2,1)} copy(bf16[4,128]{1,0:T(4,128)(2,1)} %get-tuple-element.5) | data formatting | bytes 2048

commit v2 on v1

--- a/solution.py
+++ b/solution.py
@@ -75,6 +75,9 @@
     st_recv_sem,
     rd_send_sem,
     rd_recv_sem,
+    up_sem,
+    down_sem,
+    pair_sem,
 ):
     sp = lax.axis_index("sp")
     tp = lax.axis_index("tp")
@@ -125,11 +128,25 @@
         pl.semaphore_signal(
             barrier, inc=1, device_id=(sp, flipped(tp, bits, b)), device_id_type=MESH
         )
-    for d in range(1, n_sp):
-        pl.semaphore_signal(
-            barrier, inc=1, device_id=(lax.rem(sp + d, n_sp), tp), device_id_type=MESH
-        )
-    pl.semaphore_wait(barrier, len(bits) + n_sp - 1)
+    z_count = n_sp // 2
+    z = lax.div(sp, 2)
+    partner = sp + 1 - 2 * lax.rem(sp, 2)
+    pl.semaphore_signal(barrier, inc=1, device_id=(partner, tp), device_id_type=MESH)
+
+    def signal_if(condition, sem, target):
+        @pl.when(condition)
+        def _():
+            pl.semaphore_signal(sem, inc=1, device_id=(target, tp), device_id_type=MESH)
+
+    def wait_if(condition, sem):
+        @pl.when(condition)
+        def _():
+            pl.semaphore_wait(sem, 1)
+
+    signal_if(z >= 1, barrier, sp - 2)
+    signal_if(z + 1 < z_count, barrier, sp + 2)
+    ends = jnp.where(z >= 1, 1, 0) + jnp.where(z + 1 < z_count, 1, 0)
+    pl.semaphore_wait(barrier, len(bits) + 1 + ends)
 
     def part(c, h):
         if h is None:
@@ -278,6 +295,14 @@
             s_fwd[:, cs] = s_fwd[:, cs] * f_scale[:, cs] + outer(v_group, f_keys[:, cs])
             s_bwd[:, cs] += outer(v_group, b_keys[:, cs])
 
+    for k in range(1, z_count - 1):
+        signal_if((z >= 1) & (z + k < z_count), up_sem.at[k], sp - 2)
+        signal_if((z + 1 < z_count) & (z >= k), down_sem.at[k], sp + 2)
+        wait_if(z + 1 + k < z_count, up_sem.at[k])
+        wait_if(z >= 1 + k, down_sem.at[k])
+    pl.semaphore_signal(pair_sem, inc=1, device_id=(partner, tp), device_id_type=MESH)
+    pl.semaphore_wait(pair_sem, 1)
+
     for copy in local:
         copy.wait()
 
@@ -415,6 +440,23 @@
         read_copy(peer(d), sp, d).wait_send()
     read_done.wait()
     state_done.wait()
+
+
+def hand_over(state, read):
+    def body(state_in, read_in, state_out, read_out):
+        state_out[...] = state_in[...]
+        read_out[...] = read_in[...]
+
+    vmem_spec = pl.BlockSpec(memory_space=pltpu.VMEM)
+    return pl.pallas_call(
+        body,
+        out_shape=(
+            jax.ShapeDtypeStruct(state.shape, state.dtype),
+            jax.ShapeDtypeStruct(read.shape, read.dtype),
+        ),
+        in_specs=[vmem_spec, vmem_spec],
+        out_specs=(vmem_spec, vmem_spec),
+    )(state, read)
 
 
 def shards(
@@ -443,7 +485,7 @@
     any_spec = pl.BlockSpec(memory_space=pl.ANY)
     dma = pltpu.SemaphoreType.DMA
     f32, bf16 = jnp.float32, jnp.bfloat16
-    return pl.pallas_call(
+    results = pl.pallas_call(
         functools.partial(kernel, n_sp, n_tp),
         out_shape=(
             jax.ShapeDtypeStruct((2, heads, r_count, DV), bf16),
@@ -487,6 +529,9 @@
             dma((n_sp,)),
             dma((n_sp,)),
             dma((n_sp,)),
+            pltpu.SemaphoreType.REGULAR((n_sp,)),
+            pltpu.SemaphoreType.REGULAR((n_sp,)),
+            pltpu.SemaphoreType.REGULAR,
         ],
         compiler_params=pltpu.CompilerParams(collective_id=0, has_side_effects=True),
     )(
@@ -501,6 +546,7 @@
         new_value,
         out_gain.reshape(1, DV),
     )
+    return hand_over(*results)
 
 
 def solution(mesh):

time: 91.9 us -> 89.1 us (0.970)
  local copies, waits for them, and re-layouts: 2.54 us -> 0 us
    unnamed x2 -> x0, local copies, waits for them, and re-layouts: 2.54 us -> none
    pallas_call x1, Pallas kernels: 88.4 us -> 86.9 us  [shards(): pl.pallas_call(functools.partial(kernel, n_sp, n_tp), out_shape=(jax.Shap...]
    pallas_call x0 -> x1, Pallas kernels: none -> 1.33 us  [hand_over(): pl.pallas_call(body, out_shape=(jax.ShapeDtypeStruct(state.shape, state.d...]
where the time goes in v2:
time: 89.1 us; the launch traced here: 88.9 us
  Pallas kernels  88.3 us (99%)
    pallas_call x1, Pallas kernels, shards(): pl.pallas_call(functools.partial(kernel, n_sp, n_tp), out_shape=(jax.Shap...  86.9 us

profile of v2, /device:TPU:0, one launch (start us, length us, event | category | flops | bytes accessed | tf_op | source)
XLA Modules:
  0.0 88.9 jit_solution(10876150464401211947)
XLA Ops:
  0.6 86.9 %shard_map.113 = (bf16[2,4,8,128]{3,2,1,0:T(8,128)(2,1)}, bf16[4,128]{1,0:T(4,128)(2,1)}) custom-call(bf16[1024,1024]{1,0:T(8,128)(2,1)} %tokens.1, bf16[4096,256]{1,0:T(8,128)(2,1)} %kw.1, bf16[4096,512]{1,0:T(8,128)(2,1)} %vw.1, bf16[2,4096,256]{2,1,0:T(8,128)(2,1)} %dw.1, f32[2,256]{1,0:T(2,128)} %bias_in.1, f32[4,1024]{1,0:T(4,128)} %bitcast.2, ...), custom_call_target="tpu_custom_call" | custom-call | tf_op jit(solution)/shard_map/pallas_call | solution.py:488
  87.6 1.3 %shard_map.114 = (bf16[2,4,8,128]{3,2,1,0:T(8,128)(2,1)}, bf16[4,128]{1,0:T(4,128)(2,1)}) custom-call(bf16[2,4,8,128]{3,2,1,0:T(8,128)(2,1)} %get-tuple-element.4.state_in, bf16[4,128]{1,0:T(4,128)(2,1)} %get-tuple-element.5.read_in), custom_call_target="tpu_custom_call" | custom-call | tf_op jit(solution)/shard_map/pallas_call | solution.py:451
